TPU v7x, 128 devices: a whole 4x4x4 slice. The times are simulated.
128 devices in a mesh: sp: 16 (over z, y), tp: 8 (over x, core).
Axes of the slice: x: 4, y: 4, z: 4, core: 2. Of those that a mesh axis runs over, the one named last changes fastest.
Arguments:
- inputs: bfloat16 [8192, 4096], P(('sp', 'tp')), may hold values from -42 to 42
- a_query_w: bfloat16 [4096, 2048], P(None, 'tp'), may hold values from -0.12570312 to 0.12570312
- a_key_w: bfloat16 [4096, 2048], P(None, 'tp'), may hold values from -0.12570312 to 0.12570312
- a_value_w: bfloat16 [4096, 2048], P(None, 'tp'), may hold values from -0.09375 to 0.09375
- b_query_w: bfloat16 [4096, 2048], P(None, 'tp'), may hold values from -0.12570312 to 0.12570312
- b_key_w: bfloat16 [4096, 512], P(None, 'tp'), may hold values from -0.12570312 to 0.12570312
- b_value_w: bfloat16 [4096, 512], P(None, 'tp'), may hold values from -0.09375 to 0.09375
- head_lambda: float32 [16], P('tp'), may hold values from 0.3 to 0.8
- head_gain: float32 [128], replicated, may hold values from 0.1 to 1.9
- sink_logit: float32 [32], P('tp'), may hold values from 2 to 7
- a_out_w: bfloat16 [2048, 4096], P('tp'), may hold values from -0.125 to 0.125
- b_out_w: bfloat16 [2048, 4096], P('tp'), may hold values from -0.625 to 0.625
Outputs:
- mixed: bfloat16 [8192, 4096], P(('sp', 'tp'))
All inputs are finite; a program needn't handle non-finite values.
Results may differ from a plain program's by a relative error of at most 0.015.
Values may be sent and summed in bfloat16 or wider, within the bound.
A program may use at most 128 MiB of HBM per device.

v0:
```python
import math
import jax
import jax.numpy as jnp
from jax import lax
from jax.sharding import PartitionSpec as P

HEAD_DIM = 64
VALUE_DIM = 128
WINDOW = 128
norm_eps = 0.0001
head_scale = 0.8
mask_fill = -1e30


def from_behind(value, axis, by):
    size = lax.axis_size(axis)
    pairs = [(i, i + by) for i in range(size) if 0 <= i + by < size]
    return lax.ppermute(value, axis, pairs)


def side_by_side(arrays, axis, dim, along):
    widths = [a.shape[along] for a in arrays]
    both = jnp.concatenate(arrays, axis=along)
    whole = lax.all_gather(both, axis, axis=dim, tiled=True)
    return tuple(jnp.split(whole, [sum(widths[:k]) for k in range(1, len(widths))], axis=along))


def key_span(row_count):
    span_rows = math.gcd(row_count, 1024)
    return span_rows


def attend_block(carried, queries, query_pos, block_keys, block_values, key_pos):
    running, totals, numerator = carried
    scores = jnp.einsum(
        "qhmd,khmd->hmqk", queries, block_keys, preferred_element_type=jnp.float32
    ) * HEAD_DIM ** (-0.5)
    allowed = query_pos[:, None] >= key_pos[None, :]
    scores = jnp.where(allowed, scores, mask_fill)
    updated = jnp.maximum(running, jnp.max(scores, axis=-1))
    weights = jnp.where(allowed, jnp.exp(scores - updated[..., None]), 0.0)
    shrink = jnp.exp(running - updated)
    totals = totals * shrink + jnp.sum(weights, axis=-1)
    numerator = numerator * shrink[..., None] + jnp.einsum(
        "hmqk,khe->hmqe",
        weights.astype(jnp.bfloat16),
        block_values,
        preferred_element_type=jnp.float32,
    )
    return (updated, totals, numerator)


def advance(states, groups, key_rows, value_rows):
    row_count = key_rows.shape[0]
    span_rows = key_span(row_count)
    local_heads = value_rows.shape[1] // VALUE_DIM
    key_rows = key_rows.reshape(row_count, local_heads, 2, HEAD_DIM)
    value_rows = value_rows.reshape(row_count, local_heads, VALUE_DIM)

    def one_span(span_index, current):
        span_start = span_index * span_rows
        block_keys = lax.dynamic_slice_in_dim(key_rows, span_start, span_rows, 0)
        block_values = lax.dynamic_slice_in_dim(value_rows, span_start, span_rows, 0)
        key_pos = span_start + jnp.arange(span_rows, dtype=jnp.int32)
        results = []
        for query_group, carried in zip(groups, current):
            queries, query_pos = query_group

            def compute(given_state, queries=queries, query_pos=query_pos):
                return attend_block(
                    given_state, queries, query_pos, block_keys, block_values, key_pos
                )

            def unchanged(given_state):
                return given_state

            results.append(lax.cond(key_pos[0] <= query_pos[-1], compute, unchanged, carried))
        return tuple(results)

    return lax.fori_loop(0, row_count // span_rows, one_span, states)


def finish_heads(carried, head_lambda, head_gain):
    running, totals, numerator = carried
    means = numerator / totals[..., None]
    difference = means[:, 0] - head_lambda[:, None, None] * means[:, 1]
    mean_square = jnp.mean(difference * difference, axis=-1, keepdims=True)
    return (difference * lax.rsqrt(mean_square + norm_eps) * head_gain * head_scale).astype(
        jnp.bfloat16
    )


def shards(
    inputs,
    a_query_w,
    a_key_w,
    a_value_w,
    b_query_w,
    b_key_w,
    b_value_w,
    head_lambda,
    head_gain,
    sink_logit,
    a_out_w,
    b_out_w,
):
    matrices = (a_query_w, a_key_w, a_value_w, b_query_w, b_key_w, b_value_w)

    def project(shard_piece):
        return jnp.concatenate(
            [
                jnp.dot(shard_piece, matrix, preferred_element_type=jnp.float32).astype(
                    jnp.bfloat16
                )
                for matrix in matrices
            ],
            axis=1,
        )

    projected = project(lax.all_gather(inputs, "tp", axis=0, tiled=True))
    seg_rows = projected.shape[0]
    column_edges = [0]
    for matrix in matrices:
        column_edges.append(column_edges[-1] + matrix.shape[1])
    a_query = projected[:, column_edges[0] : column_edges[1]]
    a_key = projected[:, column_edges[1] : column_edges[2]]
    a_value = projected[:, column_edges[2] : column_edges[3]]
    b_query = projected[:, column_edges[3] : column_edges[4]]
    b_pair = projected[:, column_edges[4] : column_edges[6]]
    local_heads = head_lambda.shape[0]
    offset = lax.axis_index("sp") * seg_rows
    positions = offset + jnp.arange(seg_rows, dtype=jnp.int32)
    query_heads = a_query.reshape(seg_rows, local_heads, 2, HEAD_DIM)
    groups = ((query_heads, positions),)
    initial = tuple(
        (
            (
                jnp.full((local_heads, 2, group_queries.shape[0]), mask_fill, jnp.float32),
                jnp.zeros((local_heads, 2, group_queries.shape[0]), jnp.float32),
                jnp.zeros((local_heads, 2, group_queries.shape[0], VALUE_DIM), jnp.float32),
            )
            for group_queries, group_pos in groups
        )
    )
    earlier = from_behind(b_pair[seg_rows - WINDOW :], "sp", 1)
    shard_piece = side_by_side((a_key, a_value), "sp", 0, 1)
    states = advance(initial, groups, shard_piece[0], shard_piece[1])
    finished = [finish_heads(carried, head_lambda, head_gain) for carried in states]
    a_heads = finished[0]
    kv_heads = b_pair.shape[1] // (2 * HEAD_DIM)
    group_size = b_query.shape[1] // HEAD_DIM // kv_heads
    extended = jnp.concatenate([earlier, b_pair], axis=0)
    near_keys = extended[:, : kv_heads * HEAD_DIM].reshape(WINDOW + seg_rows, kv_heads, HEAD_DIM)
    near_values = extended[:, kv_heads * HEAD_DIM :].reshape(WINDOW + seg_rows, kv_heads, HEAD_DIM)
    window_queries = b_query.reshape(seg_rows, kv_heads, group_size, HEAD_DIM)
    sink_term = sink_logit.reshape(kv_heads, group_size)[:, :, None]
    query_span = math.gcd(seg_rows, 512)
    scores = jnp.einsum(
        "qhgd,khd->hgqk", window_queries, near_keys, preferred_element_type=jnp.float32
    ) * HEAD_DIM ** (-0.5)
    query_pos = offset + 0 + jnp.arange(query_span, dtype=jnp.int32)
    near_pos = offset + 0 - WINDOW + jnp.arange(query_span + WINDOW, dtype=jnp.int32)
    distance = query_pos[:, None] - near_pos[None, :]
    allowed = (distance >= 0) & (distance < WINDOW) & (near_pos[None, :] >= 0)
    scores = jnp.where(allowed, scores, mask_fill)
    row_top = jnp.maximum(jnp.max(scores, axis=-1), sink_term)
    weights = jnp.where(allowed, jnp.exp(scores - row_top[..., None]), 0.0)
    row_total = jnp.sum(weights, axis=-1) + jnp.exp(sink_term - row_top)
    probs = (weights / row_total[..., None]).astype(jnp.bfloat16)
    block_out = jnp.einsum("hgqk,khd->qhgd", probs, near_values, preferred_element_type=jnp.float32)
    outputs = block_out.astype(jnp.bfloat16).reshape(query_span, kv_heads * group_size * HEAD_DIM)
    a_weight = a_out_w.reshape(local_heads, VALUE_DIM, a_out_w.shape[1])
    return lax.psum_scatter(
        (
            jnp.einsum("hqe,hen->qn", a_heads, a_weight, preferred_element_type=jnp.float32)
            + jnp.dot(outputs, b_out_w, preferred_element_type=jnp.float32)
        ).astype(jnp.bfloat16),
        "tp",
        scatter_dimension=0,
        tiled=True,
    )


def solution(mesh):
    return jax.shard_map(
        shards,
        mesh=mesh,
        in_specs=(
            P(("sp", "tp"), None),
            P(None, "tp"),
            P(None, "tp"),
            P(None, "tp"),
            P(None, "tp"),
            P(None, "tp"),
            P(None, "tp"),
            P("tp"),
            P(),
            P("tp"),
            P("tp", None),
            P("tp", None),
        ),
        out_specs=P(("sp", "tp"), None),
        check_vma=False,
    )
```

profile of v0, /device:TPU:0, one launch (start us, length us, event | category | flops | bytes accessed | tf_op | source)
XLA Modules:
  0.0 288.8 jit_solution(3257539258130049300)
XLA Ops:
  6.5 0.7 all-gather.3.cloned.1.call-update
  7.3 36.3 %all-gather.3.cloned.1.call-done = bf16[512,4096]{1,0:T(8,128)(2,1)} async-done(((bf16[64,4096]{1,0:T(8,128)(2,1)}), bf16[512,4096]{1,0:T(8,128)(2,1)}) %all-gather.3.cloned.1.call-update) | async-done | bytes 4194320 | tf_op jit(solution)/shard_map/all_gather | solution.py:120
  43.6 4.3 %convolution_convert_fusion.2 = bf16[512,256]{0,1:T(8,128)(2,1)S(1)} fusion(bf16[512,4096]{1,0:T(8,128)(2,1)} %all-gather.3.cloned.1.call-done, bf16[4096,256]{1,0:T(8,128)(2,1)} %param.19), kind=kOutput, calls=%fused_computation.37 | convolution fusion | flops 1073872896 | bytes 6553600 | tf_op jit(solution)/shard_map/dot_general | solution.py:112
  48.3 1.3 convolution_convert_fusion.3
  49.6 0.8 pad_maximum_fusion
  51.0 3.8 %convolution_convert_fusion.4 = bf16[512,64]{0,1:T(8,128)(2,1)S(1)} fusion(bf16[512,4096]{1,0:T(8,128)(2,1)} %all-gather.3.cloned.1.call-done, bf16[4096,64]{0,1:T(8,128)(2,1)S(1)} %copy-done.4), kind=kOutput, calls=%fused_computation.39 | convolution fusion | flops 268468224 | bytes 4784128 | tf_op jit(solution)/shard_map/dot_general | solution.py:112
  54.9 1.4 convolution_convert_fusion.5
  56.3 3.5 %collective-permute-start = (bf16[128,128]{0,1:T(8,128)(2,1)S(1)}, bf16[128,128]{0,1:T(8,128)(2,1)S(1)}, u32[]{:S(2)}, u32[]{:S(2)}) collective-permute-start(bf16[128,128]{0,1:T(8,128)(2,1)S(1)} %pad_maximum_fusion.1), channel_id=1, source_target_pairs={{0,8},{8,16},{16,24},{24,32},{32,40},{40,48},{48,56},{56,64},{64,7... | collective-permute-start | bytes 98312 | tf_op jit(solution)/shard_map/ppermute | solution.py:18
  59.8 1.3 convolution_convert_fusion
  61.2 2.0 convolution_convert_fusion.1
  63.2 1.0 fusion.19
  64.3 1.3 fusion.20
  65.7 1.8 fusion.25
  67.6 60.4 %all-gather.5.cloned.1.call-done = bf16[8192,512]{0,1:T(8,128)(2,1)} async-done(((bf16[512,512]{0,1:T(8,128)(2,1)}), bf16[8192,512]{0,1:T(8,128)(2,1)}) %all-gather.5.cloned.1.call-update) | async-done | bytes 8388624 | tf_op jit(solution)/shard_map/all_gather | solution.py:24
  128.0 5.9 %fusion.40 = (bf16[8192,256]{0,1:T(8,128)(2,1)}, bf16[8192,256]{0,1:T(8,128)(2,1)}) fusion(bf16[8192,512]{0,1:T(8,128)(2,1)} %all-gather.5.cloned.1.call-done), kind=kLoop, calls=%fused_computation.68 | loop fusion | bytes 16777216 | tf_op jit(solution)/shard_map/split | solution.py:25
  133.9 6.3 %copy.14 = bf16[8192,2,128]{2,0,1:T(8,128)(2,1)} copy(bf16[8192,2,128]{0,2,1:T(8,128)(2,1)} %bitcast.105) | data formatting | bytes 8388608 | tf_op jit(solution)/shard_map/while | solution.py:80
  140.3 31.0 %while.17 = (s32[]{:T(128)}, f32[2,2,512]{2,1,0:T(2,128)S(1)}, f32[2,2,512]{2,1,0:T(2,128)S(1)}, f32[2,2,512,128]{3,2,1,0:T(8,128)S(1)}, s32[512]{0:T(512)S(1)},...) while((s32[]{:T(128)}, f32[2,2,512]{2,1,0:T(2,128)S(1)}, ...), condition=%wide.region_5.6_spmd, body=%wide.region_0.5_spmd.sunk | while | flops 833623040 | bytes 30812476 | solution.py:80
  142.9 9.8 %conditional.2 = ((f32[2,2,512]{2,1,0:T(2,128)S(1)}, f32[2,2,512]{2,1,0:T(2,128)S(1)}, f32[2,2,512,128]{3,2,1,0:T(8,128)S(1)})) conditional(s32[]{:T(128)} %bitcast.103, (f32[2,2,512]{2,1,0:T(2,128)S(1)}, f32[2,2,512]{2,1,0:T(2,128)S(1)}, f32[2,2,512,128]{3,2,1,0:T(8,128)S(1)}) %tuple.51, (s32[512]{0:T(512)S(1)}, s32[1024]{0:T(1024)S(1)}, s32[]{:T(128)}, ...), branch_computations={%region_1.0_spmd, %region_2.4_spmd} | conditional | flops 833622016 | bytes 30808138 | solution.py:77
  143.3 2.7 fusion
  146.1 2.1 fusion.2
  148.2 4.5 %fusion.6 = f32[2,2,512,128]{3,2,1,0:T(8,128)S(1)} fusion(f32[2,2,1024,512]{3,2,1,0:T(8,128)S(1)} %get-tuple-element.290, f32[2,2,512]{2,1,0:T(2,128)S(1)} %max.21, pred[512,1024]{0,1:T(8,128)(4,1)S(1)} %broadcast_compare_fusion, f32[2,2,512,128]{3,2,1,0:T(8,128)S(1)} %get-tuple-element.245, bf16[8192,2,128]{2,0,1:T(8,128)(2,1)} %get-tuple-element.246, ...), kind=kOutput, calls=%fused_computation.7 | convolution fusion | flops 547880960 | bytes 11550724 | tf_op jit(solution)/shard_map/while/body/eval_jaxpr/cond/branch_1_fun/hmqk,khe->hmqe/dot_general | solution.py:44
  172.0 1.3 fusion.30
  173.6 3.3 %fusion.18 = bf16[512,4096]{1,0:T(8,128)(2,1)} fusion(f32[512,4096,1]{1,0,2:T(8,128)S(1)} %fusion.30, bf16[512,256]{0,1:T(8,128)(2,1)S(1)} %bitcast.107, bf16[256,4096]{1,0:T(8,128)(2,1)S(1)} %copy-done.3), kind=kOutput, calls=%fused_computation.22 | convolution fusion | flops 1077936128 | bytes 14942208 | tf_op jit(solution)/shard_map/dot_general | solution.py:176
  176.9 105.4 %reduce-scatter.2.cloned.1.call-done = bf16[64,4096]{1,0:T(8,128)(2,1)} async-done(((bf16[512,4096]{1,0:T(8,128)(2,1)}), bf16[64,4096]{1,0:T(8,128)(2,1)}) %reduce-scatter.2.cloned.1.call-update) | async-done | bytes 524304 | tf_op jit(solution)/shard_map/reduce_scatter | solution.py:173
  (79 shorter events, 12.6 us)
Async XLA Ops:
  6.5 165.5 %copy-start = (bf16[256,4096]{1,0:T(8,128)(2,1)S(1)}, bf16[256,4096]{1,0:T(8,128)(2,1)}, u32[]{:S(2)}) copy-start(bf16[256,4096]{1,0:T(8,128)(2,1)} %param.26) | copy-start | bytes 6291460
  6.5 37.0 %all-gather.3.cloned.1.call-start = ((), (), s32[]{:S(2)}) async-start(), calls=%async_computation.1 | async-start | bytes 4718592 | tf_op jit(solution)/shard_map/all_gather | solution.py:120
  7.3 120.7 %all-gather.5.cloned.1.call-start = ((), (), s32[]{:S(2)}) async-start(), calls=%async_computation.2 | async-start | bytes 8912896 | tf_op jit(solution)/shard_map/all_gather | solution.py:24
  43.6 4.3 %copy-start.1 = (bf16[512,4096]{1,0:T(8,128)(2,1)S(1)}, bf16[512,4096]{1,0:T(8,128)(2,1)}, u32[]{:S(2)}) copy-start(bf16[512,4096]{1,0:T(8,128)(2,1)} %all-gather.3.cloned.1.call-done) | copy-start | bytes 12582916
  43.6 4.7 %copy-start.9 = (bf16[4096,256]{1,0:T(8,128)(2,1)S(1)}, bf16[4096,256]{1,0:T(8,128)(2,1)}, u32[]{:S(2)}) copy-start(bf16[4096,256]{1,0:T(8,128)(2,1)} %param.18) | copy-start | bytes 6291460
  48.3 2.7 copy-start.4
  49.6 5.2 %copy-start.5 = (bf16[4096,64]{0,1:T(8,128)(2,1)S(1)}, bf16[4096,64]{0,1:T(8,128)(2,1)}, u32[]{:S(2)}) copy-start(bf16[4096,64]{0,1:T(8,128)(2,1)} %param.21) | copy-start | bytes 1572868
  50.5 231.8 %reduce-scatter.2.cloned.1.call-start = ((), (), s32[]{:S(2)}) async-start(), calls=%async_computation.3 | async-start | bytes 4718592 | tf_op jit(solution)/shard_map/reduce_scatter | solution.py:173
  50.5 4.3 %copy-start.2 = (bf16[512,4096]{1,0:T(8,128)(2,1)S(1)}, bf16[512,4096]{1,0:T(8,128)(2,1)}, u32[]{:S(2)}) copy-start(bf16[512,4096]{1,0:T(8,128)(2,1)} %all-gather.3.cloned.1.call-done) | copy-start | bytes 12582916
  51.0 8.8 %copy-start.10 = (bf16[4096,256]{1,0:T(8,128)(2,1)S(1)}, bf16[4096,256]{1,0:T(8,128)(2,1)}, u32[]{:S(2)}) copy-start(bf16[4096,256]{1,0:T(8,128)(2,1)} %param.20) | copy-start | bytes 6291460
  56.3 4.9 %copy-start.11 = (bf16[4096,256]{1,0:T(8,128)(2,1)S(1)}, bf16[4096,256]{1,0:T(8,128)(2,1)}, u32[]{:S(2)}) copy-start(bf16[4096,256]{1,0:T(8,128)(2,1)} %param.17) | copy-start | bytes 6291460
  56.3 6.9 %collective-permute-start = (bf16[128,128]{0,1:T(8,128)(2,1)S(1)}, bf16[128,128]{0,1:T(8,128)(2,1)S(1)}, u32[]{:S(2)}, u32[]{:S(2)}) collective-permute-start(bf16[128,128]{0,1:T(8,128)(2,1)S(1)} %pad_maximum_fusion.1), channel_id=1, source_target_pairs={{0,8},{8,16},{16,24},{24,32},{32,40},{40,48},{48,56},{56,64},{64,7... | collective-permute-start | bytes 98312 | tf_op jit(solution)/shard_map/ppermute | solution.py:18
  63.2 1.1 copy-start.8
  140.3 31.4 %copy-start.6 = (f32[2]{0:T(128)S(1)}, f32[2]{0:T(128)}, u32[]{:S(2)}) copy-start(f32[2]{0:T(128)} %param.23) | copy-start | bytes 28
  140.3 31.7 %copy-start.7 = (f32[128]{0:T(128)S(1)}, f32[128]{0:T(128)}, u32[]{:S(2)}) copy-start(f32[128]{0:T(128)} %param.24) | copy-start | bytes 1540
  172.0 1.6 copy-start.3
Sparse Core Ops, SparseCore 0:
  9.0 34.4 all-gather.2
  50.6 77.3 all-gather.4
  177.0 105.1 reduce-scatter.1
where the time goes:
time: 290 us; the launch traced here: 289 us
  waiting for transfers between devices  203 us (70%)
  matrix products  28.8 us (10%)
  local copies, waits for them, and re-layouts  23 us (8%)
  between operations  13.4 us (5%)
  loops' own time  11.3 us (4%)
  other arithmetic  5.89 us (2%)
  starting transfers between devices  3.61 us (1%)
    reduce_scatter x1, waiting for transfers between devices, shards(): lax.psum_scatter((jnp.einsum('hqe,hen->qn', a_heads, a_weight, preferred_...  105 us
    all_gather x1, waiting for transfers between devices, side_by_side(): whole = lax.all_gather(both, axis, axis=dim, tiled=True)  60.4 us
    all_gather x1, waiting for transfers between devices, shards(): projected = project(lax.all_gather(inputs, 'tp', axis=0, tiled=True))  36.3 us
    dot_general x6, matrix products, project(): jnp.dot(shard_piece, matrix, preferred_element_type=jnp.float32)  14.1 us
    another operation x1, loops' own time, advance(): return lax.fori_loop(0, row_count // span_rows, one_span, states)  11.2 us
    while x1, local copies, waits for them, and re-layouts, advance(): return lax.fori_loop(0, row_count // span_rows, one_span, states)  6.32 us
    split x1, local copies, waits for them, and re-layouts, side_by_side(): jnp.split(whole, [sum(widths[:k]) for k in range(1, len(widths))], axis=a...  5.86 us
  transfers between devices with their start and end apart: 4, of which 3 were waited for; matrix products, arithmetic and copies ran while one was open for 5% of the time, Pallas kernels for 0%

commit v1 on v0

--- a/solution.py
+++ b/solution.py
@@ -3,6 +3,7 @@
 import jax.numpy as jnp
 from jax import lax
 from jax.sharding import PartitionSpec as P
+from jax.lax import axis_index, axis_size, ppermute
 
 HEAD_DIM = 64
 VALUE_DIM = 128
@@ -10,6 +11,21 @@
 norm_eps = 0.0001
 head_scale = 0.8
 mask_fill = -1e30
+
+
+def _spread_stops_all(chip_axis, mat, dim_at):
+    ready, current_value = (axis_size(chip_axis), axis_index(chip_axis))
+    raw_out, z = (mat, 1)
+    while z < ready:
+        buffers = []
+        for src_i in range(ready):
+            buffers.append((src_i, src_i ^ z))
+        k_now = ppermute(raw_out, chip_axis, buffers)
+        mid_arr = jnp.concatenate([raw_out, k_now], dim_at)
+        y2 = jnp.concatenate([k_now, raw_out], dim_at)
+        raw_out = jnp.where(current_value & z == 0, mid_arr, y2)
+        z = 2 * z
+    return raw_out
 
 
 def from_behind(value, axis, by):
@@ -117,7 +133,7 @@
             axis=1,
         )
 
-    projected = project(lax.all_gather(inputs, "tp", axis=0, tiled=True))
+    projected = project(_spread_stops_all("tp", inputs, 0))
     seg_rows = projected.shape[0]
     column_edges = [0]
     for matrix in matrices:

time: 290 us -> 340 us (1.17)
  waiting for transfers between devices: 203 us -> 230 us
  matrix products: 28.8 us -> 42.9 us
  other arithmetic: 5.89 us -> 11.4 us
  starting transfers between devices: 3.61 us -> 8.77 us
    ppermute x0 -> x3, waiting for transfers between devices: none -> 71.5 us  [_spread_stops_all(): k_now = ppermute(raw_out, chip_axis, buffers)]
    all_gather x1 -> x0, waiting for transfers between devices: 36.3 us -> none  [shards(): projected = project(lax.all_gather(inputs, 'tp', axis=0, tiled=True))]
    dot_general x6, matrix products: 14.1 us -> 28.2 us  [project(): jnp.dot(shard_piece, matrix, preferred_element_type=jnp.float32)]
    all_gather x1, waiting for transfers between devices: 60.4 us -> 52.9 us  [side_by_side(): whole = lax.all_gather(both, axis, axis=dim, tiled=True)]
    select_n x0 -> x2, other arithmetic: none -> 5.54 us  [_spread_stops_all(): raw_out = jnp.where(current_value & z == 0, mid_arr, y2)]
    ppermute x0 -> x3, starting transfers between devices: none -> 4.82 us  [_spread_stops_all(): k_now = ppermute(raw_out, chip_axis, buffers)]
  transfers between devices with their start and end apart: 4 -> 6, of which waited for: 3 -> 5; matrix products, arithmetic and copies ran while one was open for 5% -> 7% of each run, Pallas kernels for 0% -> 0%
where the time goes in v1:
time: 340 us; the launch traced here: 339 us
  waiting for transfers between devices  230 us (68%)
  matrix products  42.9 us (13%)
  local copies, waits for them, and re-layouts  22 us (6%)
  between operations  13.7 us (4%)
  other arithmetic  11.4 us (3%)
  loops' own time  10.6 us (3%)
  starting transfers between devices  8.77 us (3%)
    reduce_scatter x1, waiting for transfers between devices, shards(): lax.psum_scatter((jnp.einsum('hqe,hen->qn', a_heads, a_weight, preferred_...  105 us
    ppermute x3, waiting for transfers between devices, _spread_stops_all(): k_now = ppermute(raw_out, chip_axis, buffers)  71.5 us
    all_gather x1, waiting for transfers between devices, side_by_side(): whole = lax.all_gather(both, axis, axis=dim, tiled=True)  52.9 us
    dot_general x6, matrix products, project(): jnp.dot(shard_piece, matrix, preferred_element_type=jnp.float32)  28.2 us
    another operation x1, loops' own time, advance(): return lax.fori_loop(0, row_count // span_rows, one_span, states)  10.5 us
  transfers between devices with their start and end apart: 6, of which 5 were waited for; matrix products, arithmetic and copies ran while one was open for 7% of the time, Pallas kernels for 0%

profile of v1, /device:TPU:0, one launch (start us, length us, event | category | flops | bytes accessed | tf_op | source)
XLA Modules:
  0.0 339.1 jit_solution(6440196751606363492)
XLA Ops:
  6.5 2.2 collective-permute-done
  8.8 1.9 maximum_select_fusion.2
  12.4 23.7 %collective-permute-done.1 = bf16[128,4096]{1,0:T(8,128)(2,1)} collective-permute-done((bf16[128,4096]{1,0:T(8,128)(2,1)S(1)}, bf16[128,4096]{1,0:T(8,128)(2,1)}, u32[]{:S(2)}, u32[]{:S(2)}) %collective-permute-start.1) | collective-permute-done | bytes 1048608 | tf_op jit(solution)/shard_map/ppermute | solution.py:23
  36.1 3.6 %maximum_select_fusion.1 = bf16[256,4096]{1,0:T(8,128)(2,1)} fusion(bf16[128,4096]{1,0:T(8,128)(2,1)} %collective-permute-done.1, bf16[128,4096]{1,0:T(8,128)(2,1)S(1)} %maximum_select_fusion.2, pred[]{:T(512)S(6)} %eq.10), kind=kLoop, calls=%fused_computation.31 | loop fusion | flops 9437184 | bytes 4194305 | tf_op jit(solution)/shard_map/jit(_where)/select_n | solution.py:26
  39.7 3.1 collective-permute-start.2
  42.9 45.5 %collective-permute-done.2 = bf16[256,4096]{1,0:T(8,128)(2,1)} collective-permute-done((bf16[256,4096]{1,0:T(8,128)(2,1)}, bf16[256,4096]{1,0:T(8,128)(2,1)}, u32[]{:S(2)}, u32[]{:S(2)}) %collective-permute-start.2) | collective-permute-done | bytes 2097184 | tf_op jit(solution)/shard_map/ppermute | solution.py:23
  88.4 5.5 %convolution_convert_fusion.2 = bf16[512,256]{0,1:T(8,128)(2,1)S(1)} fusion(bf16[4096,256]{1,0:T(8,128)(2,1)} %param.19, bf16[256,4096]{1,0:T(8,128)(2,1)} %collective-permute-done.2, bf16[256,4096]{1,0:T(8,128)(2,1)} %maximum_select_fusion.1, pred[]{:T(512)S(6)} %eq.9), kind=kOutput, calls=%fused_computation.39 | convolution fusion | flops 1092747264 | bytes 6553601 | tf_op jit(solution)/shard_map/dot_general | solution.py:128
  93.9 4.4 %convolution_convert_fusion.3 = bf16[512,256]{0,1:T(8,128)(2,1)S(1)} fusion(bf16[4096,256]{1,0:T(8,128)(2,1)S(1)} %copy-done.5, bf16[256,4096]{1,0:T(8,128)(2,1)} %collective-permute-done.2, bf16[256,4096]{1,0:T(8,128)(2,1)} %maximum_select_fusion.1, pred[]{:T(512)S(6)} %eq.9), kind=kOutput, calls=%fused_computation.40 | convolution fusion | flops 1092747264 | bytes 6553601 | tf_op jit(solution)/shard_map/dot_general | solution.py:128
  99.8 4.3 %convolution_convert_fusion.5 = bf16[512,64]{0,1:T(8,128)(2,1)S(1)} fusion(bf16[4096,64]{0,1:T(8,128)(2,1)S(1)} %copy-done.8, bf16[256,4096]{1,0:T(8,128)(2,1)} %collective-permute-done.2, bf16[256,4096]{1,0:T(8,128)(2,1)} %maximum_select_fusion.1, pred[]{:T(512)S(6)} %eq.9), kind=kOutput, calls=%fused_computation.42 | convolution fusion | flops 287342592 | bytes 4784129 | tf_op jit(solution)/shard_map/dot_general | solution.py:128
  104.1 4.3 %convolution_convert_fusion.4 = bf16[512,64]{0,1:T(8,128)(2,1)S(1)} fusion(bf16[4096,64]{0,1:T(8,128)(2,1)S(1)} %copy-done.9, bf16[256,4096]{1,0:T(8,128)(2,1)} %collective-permute-done.2, bf16[256,4096]{1,0:T(8,128)(2,1)} %maximum_select_fusion.1, pred[]{:T(512)S(6)} %eq.9), kind=kOutput, calls=%fused_computation.41 | convolution fusion | flops 287342592 | bytes 4784129 | tf_op jit(solution)/shard_map/dot_general | solution.py:128
  108.5 3.9 %collective-permute-start.3 = (bf16[128,128]{0,1:T(8,128)(2,1)S(1)}, bf16[128,128]{0,1:T(8,128)(2,1)S(1)}, u32[]{:S(2)}, u32[]{:S(2)}) collective-permute-start(bf16[128,128]{0,1:T(8,128)(2,1)S(1)} %pad_maximum_fusion.1), channel_id=1, source_target_pairs={{0,8},{8,16},{16,24},{24,32},{32,40},{40,48},{48,56},{56,64},{64,7... | collective-permute-start | bytes 98312 | tf_op jit(solution)/shard_map/ppermute | solution.py:34
  112.4 5.2 %convolution_convert_fusion.1 = bf16[512,256]{0,1:T(8,128)(2,1)} fusion(bf16[4096,256]{1,0:T(8,128)(2,1)S(1)} %copy-done.6, bf16[256,4096]{1,0:T(8,128)(2,1)} %collective-permute-done.2, bf16[256,4096]{1,0:T(8,128)(2,1)} %maximum_select_fusion.1, pred[]{:T(512)S(6)} %eq.9), kind=kOutput, calls=%fused_computation.38 | convolution fusion | flops 1092747264 | bytes 6553601 | tf_op jit(solution)/shard_map/dot_general | solution.py:128
  117.6 4.4 %convolution_convert_fusion = bf16[512,256]{0,1:T(8,128)(2,1)S(1)} fusion(bf16[4096,256]{1,0:T(8,128)(2,1)S(1)} %copy-done.7, bf16[256,4096]{1,0:T(8,128)(2,1)} %collective-permute-done.2, bf16[256,4096]{1,0:T(8,128)(2,1)} %maximum_select_fusion.1, pred[]{:T(512)S(6)} %eq.9), kind=kOutput, calls=%fused_computation.37 | convolution fusion | flops 1092747264 | bytes 6553601 | tf_op jit(solution)/shard_map/dot_general | solution.py:128
  124.6 1.8 fusion.25
  126.4 52.9 %all-gather.2.cloned.1.call-done = bf16[8192,512]{0,1:T(8,128)(2,1)} async-done(((bf16[512,512]{0,1:T(8,128)(2,1)}), bf16[8192,512]{0,1:T(8,128)(2,1)}) %all-gather.2.cloned.1.call-update) | async-done | bytes 8388624 | tf_op jit(solution)/shard_map/all_gather | solution.py:40
  179.3 5.9 %fusion.40 = (bf16[8192,256]{0,1:T(8,128)(2,1)}, bf16[8192,256]{0,1:T(8,128)(2,1)}) fusion(bf16[8192,512]{0,1:T(8,128)(2,1)} %all-gather.2.cloned.1.call-done), kind=kLoop, calls=%fused_computation.71 | loop fusion | bytes 16777216 | tf_op jit(solution)/shard_map/split | solution.py:41
  185.2 6.3 %copy.14 = bf16[8192,2,128]{2,0,1:T(8,128)(2,1)} copy(bf16[8192,2,128]{0,2,1:T(8,128)(2,1)} %bitcast.99) | data formatting | bytes 8388608 | tf_op jit(solution)/shard_map/while | solution.py:96
  191.6 29.7 %while.17 = (s32[]{:T(128)}, f32[2,2,512]{2,1,0:T(2,128)S(1)}, f32[2,2,512]{2,1,0:T(2,128)S(1)}, f32[2,2,512,128]{3,2,1,0:T(8,128)S(1)}, s32[512]{0:T(512)S(1)},...) while((s32[]{:T(128)}, f32[2,2,512]{2,1,0:T(2,128)S(1)}, ...), condition=%wide.region_5.6_spmd, body=%wide.region_0.5_spmd.sunk | while | flops 833623040 | bytes 30812476 | solution.py:96
  194.3 9.8 %conditional.2 = ((f32[2,2,512]{2,1,0:T(2,128)S(1)}, f32[2,2,512]{2,1,0:T(2,128)S(1)}, f32[2,2,512,128]{3,2,1,0:T(8,128)S(1)})) conditional(s32[]{:T(128)} %bitcast.97, (f32[2,2,512]{2,1,0:T(2,128)S(1)}, f32[2,2,512]{2,1,0:T(2,128)S(1)}, f32[2,2,512,128]{3,2,1,0:T(8,128)S(1)}) %tuple.51, (s32[512]{0:T(512)S(1)}, s32[1024]{0:T(1024)S(1)}, s32[]{:T(128)}, ...), branch_computations={%region_1.1_spmd, %region_2.4_spmd} | conditional | flops 833622016 | bytes 30808138 | solution.py:93
  194.7 2.7 fusion
  197.4 2.1 fusion.2
  199.6 4.5 %fusion.6 = f32[2,2,512,128]{3,2,1,0:T(8,128)S(1)} fusion(f32[2,2,1024,512]{3,2,1,0:T(8,128)S(1)} %get-tuple-element.290, f32[2,2,512]{2,1,0:T(2,128)S(1)} %max.21, pred[512,1024]{0,1:T(8,128)(4,1)S(1)} %broadcast_compare_fusion, f32[2,2,512,128]{3,2,1,0:T(8,128)S(1)} %get-tuple-element.245, bf16[8192,2,128]{2,0,1:T(8,128)(2,1)} %get-tuple-element.246, ...), kind=kOutput, calls=%fused_computation.7 | convolution fusion | flops 547880960 | bytes 11550724 | tf_op jit(solution)/shard_map/while/body/eval_jaxpr/cond/branch_1_fun/hmqk,khe->hmqe/dot_general | solution.py:60
  223.6 3.3 fusion.18
  226.9 105.3 %reduce-scatter.2.cloned.1.call-done = bf16[64,4096]{1,0:T(8,128)(2,1)} async-done(((bf16[512,4096]{1,0:T(8,128)(2,1)}), bf16[64,4096]{1,0:T(8,128)(2,1)}) %reduce-scatter.2.cloned.1.call-update) | async-done | bytes 524304 | tf_op jit(solution)/shard_map/reduce_scatter | solution.py:189
  (80 shorter events, 17.7 us)
Async XLA Ops:
  6.5 215.4 %copy-start = (bf16[256,4096]{1,0:T(8,128)(2,1)S(1)}, bf16[256,4096]{1,0:T(8,128)(2,1)}, u32[]{:S(2)}) copy-start(bf16[256,4096]{1,0:T(8,128)(2,1)} %param.26) | copy-start | bytes 6291460
  6.5 172.8 %all-gather.2.cloned.1.call-start = ((), (), s32[]{:S(2)}) async-start(), calls=%async_computation.1 | async-start | bytes 8912896 | tf_op jit(solution)/shard_map/all_gather | solution.py:40
  6.5 2.3 collective-permute-start
  10.7 25.4 %collective-permute-start.1 = (bf16[128,4096]{1,0:T(8,128)(2,1)S(1)}, bf16[128,4096]{1,0:T(8,128)(2,1)}, u32[]{:S(2)}, u32[]{:S(2)}) collective-permute-start(bf16[128,4096]{1,0:T(8,128)(2,1)S(1)} %maximum_select_fusion.2), channel_id=1, source_target_pairs={{0,2},{1,3},{2,0},{3,1},{4,6},{5,7},{6,4},{7,5},{8,10},{9,11},{10,... | collective-permute-start | bytes 3145736 | tf_op jit(solution)/shard_map/ppermute | solution.py:23
  39.7 48.6 %collective-permute-start.2 = (bf16[256,4096]{1,0:T(8,128)(2,1)}, bf16[256,4096]{1,0:T(8,128)(2,1)}, u32[]{:S(2)}, u32[]{:S(2)}) collective-permute-start(bf16[256,4096]{1,0:T(8,128)(2,1)} %maximum_select_fusion.1), channel_id=1, source_target_pairs={{0,4},{1,5},{2,6},{3,7},{4,0},{5,1},{6,2},{7,3},{8,12},{9,13},{10,... | collective-permute-start | bytes 6291464 | tf_op jit(solution)/shard_map/ppermute | solution.py:23
  42.9 51.0 %copy-start.5 = (bf16[4096,256]{1,0:T(8,128)(2,1)S(1)}, bf16[4096,256]{1,0:T(8,128)(2,1)}, u32[]{:S(2)}) copy-start(bf16[4096,256]{1,0:T(8,128)(2,1)} %param.18) | copy-start | bytes 6291460
  93.9 5.8 %copy-start.8 = (bf16[4096,64]{0,1:T(8,128)(2,1)S(1)}, bf16[4096,64]{0,1:T(8,128)(2,1)}, u32[]{:S(2)}) copy-start(bf16[4096,64]{0,1:T(8,128)(2,1)} %param.21) | copy-start | bytes 1572868
  99.2 233.0 %reduce-scatter.2.cloned.1.call-start = ((), (), s32[]{:S(2)}) async-start(), calls=%async_computation.2 | async-start | bytes 4718592 | tf_op jit(solution)/shard_map/reduce_scatter | solution.py:189
  99.8 4.3 %copy-start.9 = (bf16[4096,64]{0,1:T(8,128)(2,1)S(1)}, bf16[4096,64]{0,1:T(8,128)(2,1)}, u32[]{:S(2)}) copy-start(bf16[4096,64]{0,1:T(8,128)(2,1)} %param.22) | copy-start | bytes 1572868
  104.1 8.3 %copy-start.6 = (bf16[4096,256]{1,0:T(8,128)(2,1)S(1)}, bf16[4096,256]{1,0:T(8,128)(2,1)}, u32[]{:S(2)}) copy-start(bf16[4096,256]{1,0:T(8,128)(2,1)} %param.17) | copy-start | bytes 6291460
  108.4 9.1 %copy-start.7 = (bf16[4096,256]{1,0:T(8,128)(2,1)S(1)}, bf16[4096,256]{1,0:T(8,128)(2,1)}, u32[]{:S(2)}) copy-start(bf16[4096,256]{1,0:T(8,128)(2,1)} %param.20) | copy-start | bytes 6291460
  108.5 13.5 %collective-permute-start.3 = (bf16[128,128]{0,1:T(8,128)(2,1)S(1)}, bf16[128,128]{0,1:T(8,128)(2,1)S(1)}, u32[]{:S(2)}, u32[]{:S(2)}) collective-permute-start(bf16[128,128]{0,1:T(8,128)(2,1)S(1)} %pad_maximum_fusion.1), channel_id=1, source_target_pairs={{0,8},{8,16},{16,24},{24,32},{32,40},{40,48},{48,56},{56,64},{64,7... | collective-permute-start | bytes 98312 | tf_op jit(solution)/shard_map/ppermute | solution.py:34
  122.0 1.1 copy-start.4
  191.6 30.1 %copy-start.2 = (f32[2]{0:T(128)S(1)}, f32[2]{0:T(128)}, u32[]{:S(2)}) copy-start(f32[2]{0:T(128)} %param.23) | copy-start | bytes 28
  191.6 30.4 %copy-start.3 = (f32[128]{0:T(128)S(1)}, f32[128]{0:T(128)}, u32[]{:S(2)}) copy-start(f32[128]{0:T(128)} %param.24) | copy-start | bytes 1540
  222.0 1.6 copy-start.1
Sparse Core Ops, SparseCore 0:
  99.3 79.9 all-gather.1
  227.0 105.1 reduce-scatter.1
